TPU v7x, 32 devices: a whole 2x2x4 slice. The times are simulated.
32 devices in a mesh: ep: 8 (over z, y), tp: 4 (over x, core).
Axes of the slice: x: 2, y: 2, z: 4, core: 2. Of those that a mesh axis runs over, the one named last changes fastest.
Arguments:
- mixer_input: bfloat16 [4096, 2048], P('ep'), may hold values from -6 to 6
- mixer_gain: bfloat16 [2048], replicated, may hold values from 0.099609375 to 1.8984375
- pool_in: bfloat16 [2048, 1024], P(None, 'tp'), may hold values from -0.125 to 0.125
- pool_map: bfloat16 [4, 256, 256], P('tp'), may hold values from -0.375 to 0.375
- pool_scale: bfloat16 [1024], P('tp'), may hold values from 0.099609375 to 1.8984375
- pool_out: bfloat16 [1024, 2048], P('tp'), may hold values from -0.1875 to 0.1875
- expert_input: bfloat16 [3072, 2048], P('ep'), may hold values from -6 to 6
- expert_gain: bfloat16 [2048], replicated, may hold values from 0.099609375 to 1.8984375
- group_router: bfloat16 [2048, 4], replicated, may hold values from -0.125 to 0.125
- expert_router: bfloat16 [2048, 8], replicated, may hold values from -0.125 to 0.125
- routes: int32 [3072, 2], P('ep'), may hold values from 0 to 7, all different within a row; in each aligned block of 96 rows (0 to 95, 96 to 191, ...) at most 48 rows name the same one
- gate_weight: bfloat16 [8, 2048, 1024], P('ep', None, 'tp'), may hold values from -0.125 to 0.125
- up_weight: bfloat16 [8, 2048, 1024], P('ep', None, 'tp'), may hold values from -0.125 to 0.125
- down_weight: bfloat16 [8, 1024, 2048], P('ep', 'tp'), may hold values from -0.1875 to 0.1875
Outputs:
- mixer_output: bfloat16 [4096, 2048], P(('ep', 'tp'))
- expert_output: bfloat16 [3072, 2048], P(('ep', 'tp'))
Inputs may be any that keep to these rules, and one draw needn't show every extreme that they name: `routes`: each row names two different experts. In each aligned block of 96 rows no expert is named more than 48 times, a bound that some block reaches.
All inputs are finite; a program needn't handle non-finite values.
Results may differ from a plain program's by a relative error of at most 0.01.
Values may be sent and summed in bfloat16 or wider, within the bound.
A program may use at most 64 MiB of HBM per device.

v0:
```python
import jax
import jax.numpy as jnp
from jax import lax
from jax.experimental import pallas as pl
from jax.experimental.pallas import tpu as pltpu
from jax.sharding import PartitionSpec as P


RIM = 15
EPS = 1e-06


def passed_along(value, axis, steps):
    count = lax.axis_size(axis)
    leading, last = (max(0, -steps), min(count, count - steps))
    return lax.ppermute(value, axis, [(source, source + steps) for source in range(leading, last)])


def swapped(value, axis, mask):
    count = lax.axis_size(axis)
    return lax.ppermute(value, axis, [(source, source ^ mask) for source in range(count)])


def masks_of(axis):
    count, masks = lax.axis_size(axis), []
    while count > 1:
        count //= 2
        masks.append(count)
    return masks


def norm_rows(values, gain):
    floats = values.astype(jnp.float32)
    scale = lax.rsqrt(jnp.mean(floats * floats, axis=-1, keepdims=True) + EPS)
    return (floats * scale * gain.astype(jnp.float32)).astype(jnp.bfloat16)


def expert_weights(rows, group_router, expert_router, named):
    group_logits = jnp.dot(rows, group_router, preferred_element_type=jnp.float32)
    expert_logits = jnp.dot(rows, expert_router, preferred_element_type=jnp.float32)
    groups = group_logits.shape[1]
    experts = expert_logits.shape[1]
    member = (
        jnp.arange(experts, dtype=jnp.int32)[:, None] // (experts // groups)
        == jnp.arange(groups, dtype=jnp.int32)[None, :]
    ).astype(jnp.float32)
    group_exp = jnp.exp(group_logits)
    group_prob = group_exp / jnp.sum(group_exp, axis=1, keepdims=True)
    expert_exp = jnp.exp(expert_logits)
    within = jnp.dot(expert_exp, member, precision=lax.Precision.HIGHEST)
    prob = expert_exp * jnp.dot(group_prob / within, member.T, precision=lax.Precision.HIGHEST)
    picked = [jnp.sum(hot * prob, axis=1, keepdims=True) for hot in named]
    return [value / (picked[0] + picked[1]) for value in picked]


def mixer_half(mixer_input, mixer_gain, pool_in, pool_map, pool_scale, pool_out):
    normed = norm_rows(mixer_input, mixer_gain)
    pooled_in = jnp.dot(normed, pool_in, preferred_element_type=jnp.float32).astype(jnp.bfloat16)
    local_rows = pooled_in.shape[0]
    groups_here = pool_map.shape[0]
    channels = pool_map.shape[1]
    border = passed_along(pooled_in[local_rows - RIM :], "ep", 1)
    padded = jnp.concatenate([border, pooled_in], axis=0).astype(jnp.float32)
    padded = padded.reshape(local_rows + RIM, groups_here, channels)
    leading = lax.axis_index("tp") * groups_here
    windows = jnp.left_shift(jnp.int32(2), leading + jnp.arange(groups_here, dtype=jnp.int32))
    window_sum = jnp.zeros((local_rows, groups_here, channels), jnp.float32)
    for offset in range(RIM + 1):
        active = (offset < windows).astype(jnp.float32)
        window_sum = (
            window_sum + padded[RIM - offset : RIM - offset + local_rows] * active[None, :, None]
        )
    position = lax.axis_index("ep") * local_rows + jnp.arange(local_rows, dtype=jnp.int32)
    counts_here = jnp.minimum(position[:, None] + 1, windows[None, :]).astype(jnp.float32)
    pooled = (window_sum / counts_here[:, :, None] - padded[RIM:]).astype(jnp.bfloat16)
    mapped = jnp.einsum("tgc,gce->tge", pooled, pool_map, preferred_element_type=jnp.float32)
    mixed_rows = (
        mapped.reshape(local_rows, groups_here * channels) * pool_scale.astype(jnp.float32)
    ).astype(jnp.bfloat16)
    return jnp.dot(mixed_rows, pool_out, preferred_element_type=jnp.float32).astype(jnp.bfloat16)


def scattered_sum(partial):
    place = lax.axis_index("tp")
    blocks = lax.axis_size("tp")
    rows, model = partial.shape
    current = partial.reshape(1, blocks, rows // blocks, model)
    for mask in reversed(masks_of("tp")):
        current = current.reshape(-1, 2, rows // blocks, model)
        bit = (place // mask) % 2
        own = lax.dynamic_index_in_dim(current, bit, 1, keepdims=False)
        other = lax.dynamic_index_in_dim(current, 1 - bit, 1, keepdims=False)
        came = swapped(other, "tp", mask)
        current = (own.astype(jnp.float32) + came.astype(jnp.float32)).astype(jnp.bfloat16)
    return current.reshape(rows // blocks, model)


def spread(shard, masks):
    pieces = [shard]
    for mask in masks:
        pieces = pieces + [swapped(piece, "tp", mask) for piece in pieces]
    return pieces


def hidden_kernel(count, *refs):
    rows_ref, out_ref = refs[0], refs[-1]
    rows = rows_ref[...]
    for index in range(count):
        gate_ref, up_ref = refs[1 + index], refs[1 + count + index]
        width = gate_ref.shape[1]
        gate = jnp.dot(rows, gate_ref[...], preferred_element_type=jnp.float32)
        upward = jnp.dot(rows, up_ref[...], preferred_element_type=jnp.float32)
        hidden = gate / (1.0 + jnp.exp(-gate)) * upward
        out_ref[:, index * width : (index + 1) * width] = hidden.astype(out_ref.dtype)


def hidden_part(rows, gates, ups):
    count = len(gates)
    width = gates[0].shape[1]
    flops = 4 * count * rows.shape[0] * rows.shape[1] * width
    return pl.pallas_call(
        lambda *refs: hidden_kernel(count, *refs),
        out_shape=jax.ShapeDtypeStruct((rows.shape[0], count * width), jnp.bfloat16),
        in_specs=[pl.BlockSpec(memory_space=pltpu.VMEM)] * (1 + 2 * count),
        out_specs=pl.BlockSpec(memory_space=pltpu.VMEM),
        cost_estimate=pl.CostEstimate(
            flops=flops, bytes_accessed=4 * count * rows.shape[1] * width, transcendentals=0
        ),
    )(rows, *gates, *ups)


def result_kernel(halves, *refs):
    out_ref = refs[-1]
    downs = refs[halves:-1]
    total, index = None, 0
    for hidden_ref in refs[:halves]:
        at = 0
        while at < hidden_ref.shape[1]:
            down_ref = downs[index]
            depth = down_ref.shape[0]
            term = jnp.dot(
                hidden_ref[:, at : at + depth], down_ref[...], preferred_element_type=jnp.float32
            )
            total = term if total is None else total + term
            at, index = at + depth, index + 1
    out_ref[...] = total.astype(out_ref.dtype)


def result_part(hiddens, downs):
    rows, columns = hiddens[0].shape[0], downs[0].shape[1]
    depth = sum(down.shape[0] for down in downs)
    return pl.pallas_call(
        lambda *refs: result_kernel(len(hiddens), *refs),
        out_shape=jax.ShapeDtypeStruct((rows, columns), jnp.bfloat16),
        in_specs=[pl.BlockSpec(memory_space=pltpu.VMEM)] * (len(hiddens) + len(downs)),
        out_specs=pl.BlockSpec(memory_space=pltpu.VMEM),
        cost_estimate=pl.CostEstimate(
            flops=2 * rows * depth * columns, bytes_accessed=2 * depth * columns, transcendentals=0
        ),
    )(*hiddens, *downs)


def on_device(
    mixer_input,
    mixer_gain,
    pool_in,
    pool_map,
    pool_scale,
    pool_out,
    expert_input,
    expert_gain,
    group_router,
    expert_router,
    routes,
    gate_weight,
    up_weight,
    down_weight,
):
    masks = masks_of("tp")
    far_mask, near_masks = masks[0], masks[1:]
    parts = 2
    columns = down_weight.shape[2] // parts
    far_gate = swapped(gate_weight, "tp", far_mask)
    far_up = swapped(up_weight, "tp", far_mask)
    own_downs = [down_weight[:, :, part * columns : (part + 1) * columns] for part in range(parts)]
    far_downs = []
    for part in range(parts):
        far_downs.append(swapped(own_downs[part], "tp", far_mask))
    near_gates = spread(gate_weight, near_masks)
    near_ups = spread(up_weight, near_masks)
    near_downs = [spread(down, near_masks) for down in own_downs]

    tp_count = lax.axis_size("tp")
    ep_count = lax.axis_size("ep")
    tp_place = lax.axis_index("tp")
    experts = expert_router.shape[1]
    held = gate_weight.shape[0]
    model = expert_input.shape[1]
    block_len = expert_input.shape[0] // tp_count
    slots = 4 * block_len // experts
    own_input = lax.dynamic_slice_in_dim(expert_input, tp_place * block_len, block_len, 0)
    own_routes = lax.dynamic_slice_in_dim(routes, tp_place * block_len, block_len, 0)
    own_rows = norm_rows(own_input, expert_gain)

    expert_ids = jnp.arange(experts, dtype=jnp.int32)[None, :]
    named = [own_routes[:, j : j + 1] == expert_ids for j in range(2)]
    either = jnp.logical_or(named[0], named[1])
    earlier = jnp.arange(block_len)[:, None] > jnp.arange(block_len)[None, :]
    before = jnp.dot(
        earlier.astype(jnp.bfloat16), either.astype(jnp.bfloat16), preferred_element_type=jnp.float32
    ).astype(jnp.int32)
    place = jnp.where(either, before, -1)
    select = (
        place.T[:, None, :] == jnp.arange(slots, dtype=jnp.int32)[None, :, None]
    ).astype(jnp.bfloat16)
    sending = jnp.dot(
        select.reshape(experts * slots, block_len), own_rows, preferred_element_type=jnp.float32
    ).astype(jnp.bfloat16)
    arrived = lax.all_to_all(sending, "ep", split_axis=0, concat_axis=0, tiled=True)

    mixer_partial = mixer_half(mixer_input, mixer_gain, pool_in, pool_map, pool_scale, pool_out)
    mixer_partial, far_gate, far_up = lax.optimization_barrier((mixer_partial, far_gate, far_up))
    far_gates = spread(far_gate, near_masks)
    far_ups = spread(far_up, near_masks)
    mixer_output = scattered_sum(mixer_partial)

    portions = arrived.reshape(ep_count, held, slots, model)
    rows = [portions[:, own].reshape(ep_count * slots, model) for own in range(held)]
    near_hidden = [
        hidden_part(rows[own], [w[own] for w in near_gates], [w[own] for w in near_ups])
        for own in range(held)
    ]
    near_hidden, far_gates, far_ups = lax.optimization_barrier((near_hidden, far_gates, far_ups))
    far_hidden = [
        hidden_part(rows[own], [w[own] for w in far_gates], [w[own] for w in far_ups])
        for own in range(held)
    ]
    last, returned = far_hidden, []
    for part in range(parts):
        last, far_down = lax.optimization_barrier((last, far_downs[part]))
        if part == 0:
            far_hidden = last
        downs = near_downs[part] + spread(far_down, near_masks)
        last = [
            result_part([near_hidden[own], far_hidden[own]], [w[own] for w in downs])
            for own in range(held)
        ]
        shaped = [value.reshape(ep_count, 1, slots, columns) for value in last]
        joined = shaped[0] if held == 1 else jnp.concatenate(shaped, axis=1)
        returned.append(
            lax.all_to_all(
                joined.reshape(ep_count * held * slots, columns),
                "ep",
                split_axis=0,
                concat_axis=0,
                tiled=True,
            )
        )

    weights = expert_weights(
        own_rows, group_router, expert_router, [hot.astype(jnp.float32) for hot in named]
    )
    slot_ids = jnp.arange(experts * slots, dtype=jnp.int32)[None, :]
    picks = []
    for hot in named:
        target = jnp.sum(jnp.where(hot, expert_ids * slots + before, 0), axis=1, keepdims=True)
        picks.append((target == slot_ids).astype(jnp.bfloat16))
    outputs = []
    for value in returned:
        combined = None
        for pick, weight in zip(picks, weights):
            term = jnp.dot(pick, value, preferred_element_type=jnp.float32) * weight
            combined = term if combined is None else combined + term
        outputs.append(combined.astype(jnp.bfloat16))
    return (mixer_output, jnp.concatenate(outputs, axis=1))


def solution(mesh):
    return jax.shard_map(
        on_device,
        mesh=mesh,
        in_specs=(
            P("ep", None),
            P(),
            P(None, "tp"),
            P("tp", None, None),
            P("tp"),
            P("tp", None),
            P("ep", None),
            P(),
            P(),
            P(),
            P("ep", None),
            P("ep", None, "tp"),
            P("ep", None, "tp"),
            P("ep", "tp", None),
        ),
        out_specs=(P(("ep", "tp"), None), P(("ep", "tp"), None)),
        check_vma=False,
    )
```

profile of v0, /device:TPU:0, one launch (start us, length us, event | category | flops | bytes accessed | tf_op | source)
XLA Modules:
  0.0 138.3 jit_solution(12595849218030304772)
XLA Ops:
  3.7 2.8 %convolution_convert_fusion.1 = bf16[384,2048]{1,0:T(8,128)(2,1)} fusion(pred[384,96]{1,0:T(32,128)(4,1)S(1)} %bitcast_compare_fusion, f32[2048]{0:T(1024)S(1)} %convert_element_type.193, f32[96]{0:T(128)S(1)} %add_rsqrt_fusion.1, bf16[384,2048]{1,0:T(8,128)(2,1)} %param.20, s32[]{:T(128)S(6)} %select_n.64), kind=kOutput, calls=%fused_computation.6 | convolution fusion | flops 152567808 | bytes 2011524 | tf_op jit(solution)/shard_map/dot_general | solution.py:216
  6.5 7.3 %all-to-all-start = ((bf16[8,48,2048]{2,1,0:T(8,128)(2,1)}), bf16[8,48,2048]{2,1,0:T(8,128)(2,1)S(1)}, u32[]{:S(2)}, u32[]{:S(2)}) async-start(bf16[8,48,2048]{2,1,0:T(8,128)(2,1)} %bitcast.63), calls=%async_computation | async-start | bytes 3145728 | tf_op jit(solution)/shard_map/all_to_all | solution.py:219
  13.9 1.6 %collective-permute-start.1 = (bf16[1,2048,256]{2,1,0:T(8,128)(2,1)}, bf16[1,2048,256]{2,1,0:T(8,128)(2,1)}, u32[]{:S(2)}, u32[]{:S(2)}) collective-permute-start(bf16[1,2048,256]{2,1,0:T(8,128)(2,1)} %param.25), channel_id=1, source_target_pairs={{0,2},{1,3},{2,0},{3,1},{4,6},{5,7},{6,4},{7,5},{8,10},{9,11},{10,... | collective-permute-start | bytes 3145736 | tf_op jit(solution)/shard_map/ppermute | solution.py:21
  16.2 2.1 %fusion = f32[512]{0:T(512)S(1)} fusion(bf16[512,2048]{1,0:T(8,128)(2,1)} %param.14), kind=kLoop, calls=%fused_computation.2 | loop fusion | flops 3145216 | bytes 2099200 | tf_op jit(solution)/shard_map/reduce_sum | solution.py:34
  18.3 2.0 %fusion.8 = bf16[512,256]{1,0:T(8,128)(2,1)S(1)} fusion(bf16[2048,256]{1,0:T(8,128)(2,1)} %param.16, bf16[512,2048]{1,0:T(8,128)(2,1)S(1)} %copy-done.3, f32[2048]{0:T(1024)S(1)} %convert_element_type.158, f32[512]{0:T(512)S(1)} %add_rsqrt_fusion), kind=kOutput, calls=%fused_computation.13 | convolution fusion | flops 541196288 | bytes 3418112 | tf_op jit(solution)/shard_map/dot_general | solution.py:58
  20.3 3.8 %collective-permute-start = (bf16[15,256]{1,0:T(8,128)(2,1)S(1)}, bf16[15,256]{1,0:T(8,128)(2,1)S(1)}, u32[]{:S(2)}, u32[]{:S(2)}) collective-permute-start(bf16[15,256]{1,0:T(8,128)(2,1)S(1)} %slice.101), channel_id=1, source_target_pairs={{0,4},{4,8},{8,12},{12,16},{16,20},{20,24},{24,28},{1,5},{5,9},{9,... | collective-permute-start | bytes 23048 | tf_op jit(solution)/shard_map/ppermute | solution.py:16
  24.3 2.3 %collective-permute-done = bf16[15,256]{1,0:T(8,128)(2,1)S(1)} collective-permute-done((bf16[15,256]{1,0:T(8,128)(2,1)S(1)}, bf16[15,256]{1,0:T(8,128)(2,1)S(1)}, u32[]{:S(2)}, u32[]{:S(2)}) %collective-permute-start) | collective-permute-done | bytes 7712 | tf_op jit(solution)/shard_map/ppermute | solution.py:16
  26.7 3.9 %convolution_convert_fusion = bf16[512,2048]{1,0:T(8,128)(2,1)} fusion(bf16[256,2048]{1,0:T(8,128)(2,1)S(1)} %copy-done, f32[256]{0:T(256)S(1)} %convert_element_type.180, f32[527,256]{1,0:T(8,128)S(1)} %maximum_convert_fusion, f32[512]{0:T(512)S(1)} %minimum_convert_fusion, f32[]{:T(128)S(6)} %convert_element_type.177, f32[]{:T(128)S(6)} %convert_element_type.176, ...), kind=kOutput, calls=%fused_computation.5 | convolution fusion | flops 609746944 | bytes 11668544 | tf_op jit(solution)/shard_map/dot_general | solution.py:80
  30.6 9.6 %collective-permute-done.1 = bf16[1,2048,256]{2,1,0:T(8,128)(2,1)} collective-permute-done((bf16[1,2048,256]{2,1,0:T(8,128)(2,1)}, bf16[1,2048,256]{2,1,0:T(8,128)(2,1)}, u32[]{:S(2)}, u32[]{:S(2)}) %collective-permute-start.1) | collective-permute-done | bytes 1048608 | tf_op jit(solution)/shard_map/ppermute | solution.py:21
  40.3 21.1 %collective-permute-done.2 = bf16[1,2048,256]{2,1,0:T(8,128)(2,1)} collective-permute-done((bf16[1,2048,256]{2,1,0:T(8,128)(2,1)}, bf16[1,2048,256]{2,1,0:T(8,128)(2,1)}, u32[]{:S(2)}, u32[]{:S(2)}) %collective-permute-start.2) | collective-permute-done | bytes 1048608 | tf_op jit(solution)/shard_map/ppermute | solution.py:21
  61.8 2.7 %slice_bitcast_fusion.3 = (bf16[256,1024]{1,0:T(8,128)(2,1)}, bf16[256,1024]{1,0:T(8,128)(2,1)}, bf16[1,256,1024]{2,1,0:T(8,128)(2,1)}, bf16[1,256,1024]{2,1,0:T(8,128)(2,1)}) fusion(bf16[1,256,2048]{2,1,0:T(8,128)(2,1)} %param.27), kind=kLoop, calls=%fused_computation.113 | loop fusion | bytes 3145728 | tf_op jit(solution)/shard_map/squeeze | solution.py:245
  64.5 1.5 %collective-permute-start.9 = (bf16[1,256,1024]{2,1,0:T(8,128)(2,1)}, bf16[1,256,1024]{2,1,0:T(8,128)(2,1)}, u32[]{:S(2)}, u32[]{:S(2)}) collective-permute-start(bf16[1,256,1024]{2,1,0:T(8,128)(2,1)} %get-tuple-element.31), channel_id=1, source_target_pairs={{0,2},{1,3},{2,0},{3,1},{4,6},{5,7},{6,4},{7,5},{8,10},{9,11},{10,... | collective-permute-start | bytes 1572872 | tf_op jit(solution)/shard_map/ppermute | solution.py:21
  67.2 5.2 %shard_map.149.refs_0_ = bf16[384,512]{1,0:T(8,128)(2,1)} custom-call(bf16[384,2048]{1,0:T(8,128)(2,1)} %bitcast.57, bf16[2048,256]{1,0:T(8,128)(2,1)} %bitcast.68, bf16[2048,256]{1,0:T(8,128)(2,1)} %bitcast.12.refs_2_, bf16[2048,256]{1,0:T(8,128)(2,1)} %bitcast.69, bf16[2048,256]{1,0:T(8,128)(2,1)} %bitcast.14.refs_4_), custom_call_target="tpu_custom_call" | custom-call | flops 1610612736 | bytes 4194304 | tf_op jit(solution)/shard_map/pallas_call | solution.py:121
  72.4 5.4 %shard_map.150.refs_1_ = bf16[384,512]{1,0:T(8,128)(2,1)} custom-call(bf16[384,2048]{1,0:T(8,128)(2,1)} %bitcast.58, bf16[2048,256]{1,0:T(8,128)(2,1)} %bitcast.15.refs_1_, bf16[2048,256]{1,0:T(8,128)(2,1)} %bitcast.16.refs_2_, bf16[2048,256]{1,0:T(8,128)(2,1)} %bitcast.17.refs_3_, bf16[2048,256]{1,0:T(8,128)(2,1)} %bitcast.18.refs_4_), custom_call_target="tpu_custom_call" | custom-call | flops 1610612736 | bytes 4194304 | tf_op jit(solution)/shard_map/pallas_call | solution.py:121
  80.2 1.5 %collective-permute-start.13 = (bf16[1,256,1024]{2,1,0:T(8,128)(2,1)}, bf16[1,256,1024]{2,1,0:T(8,128)(2,1)}, u32[]{:S(2)}, u32[]{:S(2)}) collective-permute-start(bf16[1,256,1024]{2,1,0:T(8,128)(2,1)} %get-tuple-element.30), channel_id=1, source_target_pairs={{0,2},{1,3},{2,0},{3,1},{4,6},{5,7},{6,4},{7,5},{8,10},{9,11},{10,... | collective-permute-start | bytes 1572872 | tf_op jit(solution)/shard_map/ppermute | solution.py:21
  83.0 3.6 %shard_map.151 = bf16[384,1024]{1,0:T(8,128)(2,1)} custom-call(bf16[384,512]{1,0:T(8,128)(2,1)} %shard_map.149.refs_0_, bf16[384,512]{1,0:T(8,128)(2,1)} %shard_map.150.refs_1_, bf16[256,1024]{1,0:T(8,128)(2,1)} %get-tuple-element.28.refs_2_, bf16[256,1024]{1,0:T(8,128)(2,1)} %bitcast.20.refs_3_, bf16[256,1024]{1,0:T(8,128)(2,1)} %bitcast.21.refs_4_, ...), custom_call_target="tpu_custom_call" | custom-call | flops 805306368 | bytes 2097152 | tf_op jit(solution)/shard_map/pallas_call | solution.py:152
  86.7 5.6 %all-to-all-start.1 = ((bf16[8,48,1024]{2,1,0:T(8,128)(2,1)}), bf16[8,48,1024]{2,1,0:T(8,128)(2,1)S(1)}, u32[]{:S(2)}, u32[]{:S(2)}) async-start(bf16[8,48,1024]{2,1,0:T(8,128)(2,1)} %bitcast.65), calls=%async_computation.1 | async-start | bytes 1572864 | tf_op jit(solution)/shard_map/all_to_all | solution.py:251
  94.9 1.6 %fusion.5 = bf16[2,128,2048]{2,1,0:T(8,128)(2,1)S(1)} fusion(bf16[2,128,2048]{2,1,0:T(8,128)(2,1)S(1)} %collective-permute-done.3, bf16[2,2,128,2048]{3,2,1,0:T(8,128)(2,1)} %bitcast.66, s32[]{:T(128)S(6)} %select_n.58), kind=kLoop, calls=%fused_computation.9 | loop fusion | flops 2097152 | bytes 3145732 | tf_op jit(solution)/shard_map/convert_element_type | solution.py:94
  98.3 1.5 %collective-permute-start.4 = (bf16[1,128,2048]{2,1,0:T(8,128)(2,1)}, bf16[1,128,2048]{2,1,0:T(8,128)(2,1)}, u32[]{:S(2)}, u32[]{:S(2)}) collective-permute-start(bf16[1,128,2048]{2,1,0:T(8,128)(2,1)} %constant_dynamic-slice_fusion.1), channel_id=1, source_target_pairs={{0,2},{1,3},{2,0},{3,1},{4,6},{5,7},{6,4},{7,5},{8,10},{9,11},{10,... | collective-permute-start | bytes 1572872 | tf_op jit(solution)/shard_map/ppermute | solution.py:21
  100.6 3.7 %shard_map.152 = bf16[384,1024]{1,0:T(8,128)(2,1)} custom-call(bf16[384,512]{1,0:T(8,128)(2,1)} %shard_map.149.refs_0_, bf16[384,512]{1,0:T(8,128)(2,1)} %shard_map.150.refs_1_, bf16[256,1024]{1,0:T(8,128)(2,1)} %get-tuple-element.29.refs_2_, bf16[256,1024]{1,0:T(8,128)(2,1)} %bitcast.70, bf16[256,1024]{1,0:T(8,128)(2,1)} %bitcast.27.refs_4_, ...), custom_call_target="tpu_custom_call" | custom-call | flops 805306368 | bytes 2097152 | tf_op jit(solution)/shard_map/pallas_call | solution.py:152
  104.3 8.6 %all-to-all-done.1 = bf16[8,48,1024]{2,1,0:T(8,128)(2,1)S(1)} async-done(((bf16[8,48,1024]{2,1,0:T(8,128)(2,1)}), bf16[8,48,1024]{2,1,0:T(8,128)(2,1)S(1)}, u32[]{:S(2)}, u32[]{:S(2)}) %all-to-all-start.1) | async-done | bytes 786464 | tf_op jit(solution)/shard_map/all_to_all | solution.py:251
  112.9 3.6 %all-to-all-start.2 = ((bf16[8,48,1024]{2,1,0:T(8,128)(2,1)}), bf16[8,48,1024]{2,1,0:T(8,128)(2,1)S(1)}, u32[]{:S(2)}, u32[]{:S(2)}) async-start(bf16[8,48,1024]{2,1,0:T(8,128)(2,1)} %bitcast.64), calls=%async_computation.2 | async-start | bytes 1572864 | tf_op jit(solution)/shard_map/all_to_all | solution.py:251
  116.8 2.1 %fusion.20 = bf16[128,2048]{1,0:T(8,128)(2,1)} fusion(bf16[1,128,2048]{2,1,0:T(8,128)(2,1)} %collective-permute-done.4, bf16[2,128,2048]{2,1,0:T(8,128)(2,1)} %copy-done.2, s32[]{:T(128)S(6)} %select_n.62), kind=kLoop, calls=%fused_computation.36 | loop fusion | flops 1048576 | bytes 1572868 | tf_op jit(solution)/shard_map/reshape | solution.py:95
  119.6 17.3 %all-to-all-done.2 = bf16[8,48,1024]{2,1,0:T(8,128)(2,1)S(1)} async-done(((bf16[8,48,1024]{2,1,0:T(8,128)(2,1)}), bf16[8,48,1024]{2,1,0:T(8,128)(2,1)S(1)}, u32[]{:S(2)}, u32[]{:S(2)}) %all-to-all-start.2) | async-done | bytes 786464 | tf_op jit(solution)/shard_map/all_to_all | solution.py:251
  (73 shorter events, 16.8 us)
Async XLA Ops:
  0.6 26.1 %copy-start = (bf16[256,2048]{1,0:T(8,128)(2,1)S(1)}, bf16[256,2048]{1,0:T(8,128)(2,1)}, u32[]{:S(2)}) copy-start(bf16[256,2048]{1,0:T(8,128)(2,1)} %param.19) | copy-start | bytes 3145732
  3.7 12.5 %copy-start.6 = (bf16[2048]{0:T(1024)(128)(2,1)S(1)}, bf16[2048]{0:T(1024)(128)(2,1)}, u32[]{:S(2)}) copy-start(bf16[2048]{0:T(1024)(128)(2,1)} %param.15) | copy-start | bytes 12292
  6.5 59.5 %all-to-all-start = ((bf16[8,48,2048]{2,1,0:T(8,128)(2,1)}), bf16[8,48,2048]{2,1,0:T(8,128)(2,1)S(1)}, u32[]{:S(2)}, u32[]{:S(2)}) async-start(bf16[8,48,2048]{2,1,0:T(8,128)(2,1)} %bitcast.63), calls=%async_computation | async-start | bytes 3145728 | tf_op jit(solution)/shard_map/all_to_all | solution.py:219
  13.9 4.4 %copy-start.3 = (bf16[512,2048]{1,0:T(8,128)(2,1)S(1)}, bf16[512,2048]{1,0:T(8,128)(2,1)}, u32[]{:S(2)}) copy-start(bf16[512,2048]{1,0:T(8,128)(2,1)} %param.14) | copy-start | bytes 6291460
  13.9 26.4 %collective-permute-start.1 = (bf16[1,2048,256]{2,1,0:T(8,128)(2,1)}, bf16[1,2048,256]{2,1,0:T(8,128)(2,1)}, u32[]{:S(2)}, u32[]{:S(2)}) collective-permute-start(bf16[1,2048,256]{2,1,0:T(8,128)(2,1)} %param.25), channel_id=1, source_target_pairs={{0,2},{1,3},{2,0},{3,1},{4,6},{5,7},{6,4},{7,5},{8,10},{9,11},{10,... | collective-permute-start | bytes 3145736 | tf_op jit(solution)/shard_map/ppermute | solution.py:21
  15.4 50.6 %collective-permute-start.5 = (bf16[1,2048,256]{2,1,0:T(8,128)(2,1)}, bf16[1,2048,256]{2,1,0:T(8,128)(2,1)}, u32[]{:S(2)}, u32[]{:S(2)}) collective-permute-start(bf16[1,2048,256]{2,1,0:T(8,128)(2,1)} %param.25), channel_id=1, source_target_pairs={{0,1},{1,0},{2,3},{3,2},{4,5},{5,4},{6,7},{7,6},{8,9},{9,8},{10,11... | collective-permute-start | bytes 3145736 | tf_op jit(solution)/shard_map/ppermute | solution.py:21
  15.4 45.9 %collective-permute-start.2 = (bf16[1,2048,256]{2,1,0:T(8,128)(2,1)}, bf16[1,2048,256]{2,1,0:T(8,128)(2,1)}, u32[]{:S(2)}, u32[]{:S(2)}) collective-permute-start(bf16[1,2048,256]{2,1,0:T(8,128)(2,1)} %param.26), channel_id=1, source_target_pairs={{0,2},{1,3},{2,0},{3,1},{4,6},{5,7},{6,4},{7,5},{8,10},{9,11},{10,... | collective-permute-start | bytes 3145736 | tf_op jit(solution)/shard_map/ppermute | solution.py:21
  16.0 50.1 %collective-permute-start.6 = (bf16[1,2048,256]{2,1,0:T(8,128)(2,1)}, bf16[1,2048,256]{2,1,0:T(8,128)(2,1)}, u32[]{:S(2)}, u32[]{:S(2)}) collective-permute-start(bf16[1,2048,256]{2,1,0:T(8,128)(2,1)} %param.26), channel_id=1, source_target_pairs={{0,1},{1,0},{2,3},{3,2},{4,5},{5,4},{6,7},{7,6},{8,9},{9,8},{10,11... | collective-permute-start | bytes 3145736 | tf_op jit(solution)/shard_map/ppermute | solution.py:21
  18.3 5.9 %copy-start.9 = (bf16[256]{0:T(256)(128)(2,1)S(1)}, bf16[256]{0:T(256)(128)(2,1)}, u32[]{:S(2)}) copy-start(bf16[256]{0:T(256)(128)(2,1)} %param.18) | copy-start | bytes 1540
  20.3 6.3 %collective-permute-start = (bf16[15,256]{1,0:T(8,128)(2,1)S(1)}, bf16[15,256]{1,0:T(8,128)(2,1)S(1)}, u32[]{:S(2)}, u32[]{:S(2)}) collective-permute-start(bf16[15,256]{1,0:T(8,128)(2,1)S(1)} %slice.101), channel_id=1, source_target_pairs={{0,4},{4,8},{8,12},{12,16},{16,20},{20,24},{24,28},{1,5},{5,9},{9,... | collective-permute-start | bytes 23048 | tf_op jit(solution)/shard_map/ppermute | solution.py:16
  61.3 11.1 %collective-permute-start.7 = (bf16[1,2048,256]{2,1,0:T(8,128)(2,1)}, bf16[1,2048,256]{2,1,0:T(8,128)(2,1)}, u32[]{:S(2)}, u32[]{:S(2)}) collective-permute-start(bf16[1,2048,256]{2,1,0:T(8,128)(2,1)} %collective-permute-done.1), channel_id=1, source_target_pairs={{0,1},{1,0},{2,3},{3,2},{4,5},{5,4},{6,7},{7,6},{8,9},{9,8},{10,11... | collective-permute-start | bytes 3145736 | tf_op jit(solution)/shard_map/ppermute | solution.py:21
  61.3 11.1 %collective-permute-start.8 = (bf16[1,2048,256]{2,1,0:T(8,128)(2,1)}, bf16[1,2048,256]{2,1,0:T(8,128)(2,1)}, u32[]{:S(2)}, u32[]{:S(2)}) collective-permute-start(bf16[1,2048,256]{2,1,0:T(8,128)(2,1)} %collective-permute-done.2), channel_id=1, source_target_pairs={{0,1},{1,0},{2,3},{3,2},{4,5},{5,4},{6,7},{7,6},{8,9},{9,8},{10,11... | collective-permute-start | bytes 3145736 | tf_op jit(solution)/shard_map/ppermute | solution.py:21
  64.5 14.1 %collective-permute-start.9 = (bf16[1,256,1024]{2,1,0:T(8,128)(2,1)}, bf16[1,256,1024]{2,1,0:T(8,128)(2,1)}, u32[]{:S(2)}, u32[]{:S(2)}) collective-permute-start(bf16[1,256,1024]{2,1,0:T(8,128)(2,1)} %get-tuple-element.31), channel_id=1, source_target_pairs={{0,2},{1,3},{2,0},{3,1},{4,6},{5,7},{6,4},{7,5},{8,10},{9,11},{10,... | collective-permute-start | bytes 1572872 | tf_op jit(solution)/shard_map/ppermute | solution.py:21
  66.0 17.0 %collective-permute-start.10 = (bf16[1,256,1024]{2,1,0:T(8,128)(2,1)}, bf16[1,256,1024]{2,1,0:T(8,128)(2,1)}, u32[]{:S(2)}, u32[]{:S(2)}) collective-permute-start(bf16[1,256,1024]{2,1,0:T(8,128)(2,1)} %get-tuple-element.31), channel_id=1, source_target_pairs={{0,1},{1,0},{2,3},{3,2},{4,5},{5,4},{6,7},{7,6},{8,9},{9,8},{10,11... | collective-permute-start | bytes 1572872 | tf_op jit(solution)/shard_map/ppermute | solution.py:21
  72.4 6.3 %copy-start.4 = (bf16[512,2048]{1,0:T(8,128)(2,1)S(1)}, bf16[512,2048]{1,0:T(8,128)(2,1)}, u32[]{:S(2)}) copy-start(bf16[512,2048]{1,0:T(8,128)(2,1)} %convolution_convert_fusion) | copy-start | bytes 6291460
  78.7 4.3 %collective-permute-start.11 = (bf16[1,256,1024]{2,1,0:T(8,128)(2,1)}, bf16[1,256,1024]{2,1,0:T(8,128)(2,1)}, u32[]{:S(2)}, u32[]{:S(2)}) collective-permute-start(bf16[1,256,1024]{2,1,0:T(8,128)(2,1)} %collective-permute-done.9), channel_id=1, source_target_pairs={{0,1},{1,0},{2,3},{3,2},{4,5},{5,4},{6,7},{7,6},{8,9},{9,8},{10,11... | collective-permute-start | bytes 1572872 | tf_op jit(solution)/shard_map/ppermute | solution.py:21
  79.7 15.2 %collective-permute-start.3 = (bf16[2,128,2048]{2,1,0:T(8,128)(2,1)}, bf16[2,128,2048]{2,1,0:T(8,128)(2,1)S(1)}, u32[]{:S(2)}, u32[]{:S(2)}) collective-permute-start(bf16[2,128,2048]{2,1,0:T(8,128)(2,1)} %dynamic-slice_bitcast_fusion), channel_id=1, source_target_pairs={{0,1},{1,0},{2,3},{3,2},{4,5},{5,4},{6,7},{7,6},{8,9},{9,8},{10,11... | collective-permute-start | bytes 3145736 | tf_op jit(solution)/shard_map/ppermute | solution.py:21
  80.2 19.6 %collective-permute-start.12 = (bf16[1,256,1024]{2,1,0:T(8,128)(2,1)}, bf16[1,256,1024]{2,1,0:T(8,128)(2,1)S(1)}, u32[]{:S(2)}, u32[]{:S(2)}) collective-permute-start(bf16[1,256,1024]{2,1,0:T(8,128)(2,1)} %get-tuple-element.30), channel_id=1, source_target_pairs={{0,1},{1,0},{2,3},{3,2},{4,5},{5,4},{6,7},{7,6},{8,9},{9,8},{10,11... | collective-permute-start | bytes 1572872 | tf_op jit(solution)/shard_map/ppermute | solution.py:21
  80.2 14.7 %collective-permute-start.13 = (bf16[1,256,1024]{2,1,0:T(8,128)(2,1)}, bf16[1,256,1024]{2,1,0:T(8,128)(2,1)}, u32[]{:S(2)}, u32[]{:S(2)}) collective-permute-start(bf16[1,256,1024]{2,1,0:T(8,128)(2,1)} %get-tuple-element.30), channel_id=1, source_target_pairs={{0,2},{1,3},{2,0},{3,1},{4,6},{5,7},{6,4},{7,5},{8,10},{9,11},{10,... | collective-permute-start | bytes 1572872 | tf_op jit(solution)/shard_map/ppermute | solution.py:21
  83.0 9.3 %copy-start.7 = (bf16[2048,8]{0,1:T(8,128)(2,1)S(1)}, bf16[2048,8]{0,1:T(8,128)(2,1)}, u32[]{:S(2)}) copy-start(bf16[2048,8]{0,1:T(8,128)(2,1)} %param.23) | copy-start | bytes 98308
  86.7 26.2 %all-to-all-start.1 = ((bf16[8,48,1024]{2,1,0:T(8,128)(2,1)}), bf16[8,48,1024]{2,1,0:T(8,128)(2,1)S(1)}, u32[]{:S(2)}, u32[]{:S(2)}) async-start(bf16[8,48,1024]{2,1,0:T(8,128)(2,1)} %bitcast.65), calls=%async_computation.1 | async-start | bytes 1572864 | tf_op jit(solution)/shard_map/all_to_all | solution.py:251
  94.9 4.9 %collective-permute-start.14 = (bf16[1,256,1024]{2,1,0:T(8,128)(2,1)}, bf16[1,256,1024]{2,1,0:T(8,128)(2,1)}, u32[]{:S(2)}, u32[]{:S(2)}) collective-permute-start(bf16[1,256,1024]{2,1,0:T(8,128)(2,1)} %collective-permute-done.13), channel_id=1, source_target_pairs={{0,1},{1,0},{2,3},{3,2},{4,5},{5,4},{6,7},{7,6},{8,9},{9,8},{10,11... | collective-permute-start | bytes 1572872 | tf_op jit(solution)/shard_map/ppermute | solution.py:21
  98.3 18.5 %collective-permute-start.4 = (bf16[1,128,2048]{2,1,0:T(8,128)(2,1)}, bf16[1,128,2048]{2,1,0:T(8,128)(2,1)}, u32[]{:S(2)}, u32[]{:S(2)}) collective-permute-start(bf16[1,128,2048]{2,1,0:T(8,128)(2,1)} %constant_dynamic-slice_fusion.1), channel_id=1, source_target_pairs={{0,2},{1,3},{2,0},{3,1},{4,6},{5,7},{6,4},{7,5},{8,10},{9,11},{10,... | collective-permute-start | bytes 1572872 | tf_op jit(solution)/shard_map/ppermute | solution.py:21
  112.9 24.0 %all-to-all-start.2 = ((bf16[8,48,1024]{2,1,0:T(8,128)(2,1)}), bf16[8,48,1024]{2,1,0:T(8,128)(2,1)S(1)}, u32[]{:S(2)}, u32[]{:S(2)}) async-start(bf16[8,48,1024]{2,1,0:T(8,128)(2,1)} %bitcast.64), calls=%async_computation.2 | async-start | bytes 1572864 | tf_op jit(solution)/shard_map/all_to_all | solution.py:251
  (4 other events, 6.9 us)
where the time goes:
time: 139 us; the launch traced here: 138 us
  waiting for transfers between devices  60.8 us (44%)
  starting transfers between devices  28.3 us (20%)
  Pallas kernels  17.9 us (13%)
  matrix products  13.2 us (9%)
  other arithmetic  8.77 us (6%)
  local copies, waits for them, and re-layouts  8.42 us (6%)
    ppermute x14, waiting for transfers between devices, swapped(): lax.ppermute(value, axis, [(source, source ^ mask) for source in range(co...  32.6 us
    all_to_all x2, waiting for transfers between devices, on_device(): lax.all_to_all(joined.reshape(ep_count * held * slots, columns), 'ep', sp...  25.9 us
    pallas_call x2, Pallas kernels, hidden_part(): pl.pallas_call(lambda *refs: hidden_kernel(count, *refs), out_shape=jax.S...  10.6 us
    all_to_all x2, starting transfers between devices, on_device(): lax.all_to_all(joined.reshape(ep_count * held * slots, columns), 'ep', sp...  9.29 us
    ppermute x14, starting transfers between devices, swapped(): lax.ppermute(value, axis, [(source, source ^ mask) for source in range(co...  7.82 us
    all_to_all x1, starting transfers between devices, on_device(): lax.all_to_all(sending, 'ep', split_axis=0, concat_axis=0, tiled=True)  7.31 us
    pallas_call x2, Pallas kernels, result_part(): pl.pallas_call(lambda *refs: result_kernel(len(hiddens), *refs), out_shap...  7.3 us
    dot_general x1, matrix products, mixer_half(): jnp.dot(mixed_rows, pool_out, preferred_element_type=jnp.float32)  3.92 us
  transfers between devices with their start and end apart: 18, of which 7 were waited for; matrix products, arithmetic and copies ran while one was open for 15% of the time, Pallas kernels for 13%

commit v1 on v0

--- a/solution.py
+++ b/solution.py
@@ -53,13 +53,10 @@
     return [value / (picked[0] + picked[1]) for value in picked]
 
 
-def mixer_half(mixer_input, mixer_gain, pool_in, pool_map, pool_scale, pool_out):
-    normed = norm_rows(mixer_input, mixer_gain)
-    pooled_in = jnp.dot(normed, pool_in, preferred_element_type=jnp.float32).astype(jnp.bfloat16)
+def mixer_half(pooled_in, border, pool_map, pool_scale, pool_out):
     local_rows = pooled_in.shape[0]
     groups_here = pool_map.shape[0]
     channels = pool_map.shape[1]
-    border = passed_along(pooled_in[local_rows - RIM :], "ep", 1)
     padded = jnp.concatenate([border, pooled_in], axis=0).astype(jnp.float32)
     padded = padded.reshape(local_rows + RIM, groups_here, channels)
     leading = lax.axis_index("tp") * groups_here
@@ -102,62 +99,104 @@
     return pieces
 
 
-def hidden_kernel(count, *refs):
-    rows_ref, out_ref = refs[0], refs[-1]
-    rows = rows_ref[...]
+def hidden_kernel(pieces, count, *refs):
+    sources, out_ref = refs[: pieces + 2 * count], refs[pieces + 2 * count]
+    rows_buf, weight_buf, sem = refs[pieces + 2 * count + 1 :]
+    length = rows_buf.shape[0] // pieces
+    targets = [rows_buf.at[pl.ds(index * length, length)] for index in range(pieces)]
+    targets += [weight_buf.at[index] for index in range(2 * count)]
+    copies = [
+        pltpu.make_async_copy(source, target, sem.at[index])
+        for index, (source, target) in enumerate(zip(sources, targets))
+    ]
+    for copy in copies:
+        copy.start()
+    for copy in copies[:pieces]:
+        copy.wait()
+    rows = rows_buf[...]
+    width = weight_buf.shape[2]
     for index in range(count):
-        gate_ref, up_ref = refs[1 + index], refs[1 + count + index]
-        width = gate_ref.shape[1]
-        gate = jnp.dot(rows, gate_ref[...], preferred_element_type=jnp.float32)
-        upward = jnp.dot(rows, up_ref[...], preferred_element_type=jnp.float32)
+        copies[pieces + 2 * index].wait()
+        gate = jnp.dot(rows, weight_buf[2 * index], preferred_element_type=jnp.float32)
+        copies[pieces + 2 * index + 1].wait()
+        upward = jnp.dot(rows, weight_buf[2 * index + 1], preferred_element_type=jnp.float32)
         hidden = gate / (1.0 + jnp.exp(-gate)) * upward
         out_ref[:, index * width : (index + 1) * width] = hidden.astype(out_ref.dtype)
 
 
-def hidden_part(rows, gates, ups):
-    count = len(gates)
-    width = gates[0].shape[1]
-    flops = 4 * count * rows.shape[0] * rows.shape[1] * width
+def hidden_part(pieces, gates, ups):
+    count, parts = len(gates), len(pieces)
+    depth, width = gates[0].shape
+    rows = parts * pieces[0].shape[0]
+    weights = [array for pair in zip(gates, ups) for array in pair]
     return pl.pallas_call(
-        lambda *refs: hidden_kernel(count, *refs),
-        out_shape=jax.ShapeDtypeStruct((rows.shape[0], count * width), jnp.bfloat16),
-        in_specs=[pl.BlockSpec(memory_space=pltpu.VMEM)] * (1 + 2 * count),
+        lambda *refs: hidden_kernel(parts, count, *refs),
+        out_shape=jax.ShapeDtypeStruct((rows, count * width), jnp.bfloat16),
+        in_specs=[pl.BlockSpec(memory_space=pl.ANY)] * (parts + 2 * count),
         out_specs=pl.BlockSpec(memory_space=pltpu.VMEM),
+        scratch_shapes=[
+            pltpu.VMEM((rows, depth), jnp.bfloat16),
+            pltpu.VMEM((2 * count, depth, width), jnp.bfloat16),
+            pltpu.SemaphoreType.DMA((parts + 2 * count,)),
+        ],
         cost_estimate=pl.CostEstimate(
-            flops=flops, bytes_accessed=4 * count * rows.shape[1] * width, transcendentals=0
+            flops=4 * count * rows * depth * width,
+            bytes_accessed=4 * count * depth * width,
+            transcendentals=0,
         ),
-    )(rows, *gates, *ups)
-
-
-def result_kernel(halves, *refs):
-    out_ref = refs[-1]
-    downs = refs[halves:-1]
+    )(*pieces, *weights)
+
+
+def result_kernel(halves, count, parts, *refs):
+    hiddens, downs = refs[:halves], refs[halves : halves + count]
+    outs = refs[halves + count : halves + count + parts]
+    down_buf, sem = refs[halves + count + parts :]
+    copies = [
+        pltpu.make_async_copy(source, down_buf.at[index], sem.at[index])
+        for index, source in enumerate(downs)
+    ]
+    for copy in copies:
+        copy.start()
+    depth = down_buf.shape[1]
     total, index = None, 0
-    for hidden_ref in refs[:halves]:
-        at = 0
-        while at < hidden_ref.shape[1]:
-            down_ref = downs[index]
-            depth = down_ref.shape[0]
+    for hidden_ref in hiddens:
+        for at in range(0, hidden_ref.shape[1], depth):
+            copies[index].wait()
             term = jnp.dot(
-                hidden_ref[:, at : at + depth], down_ref[...], preferred_element_type=jnp.float32
+                hidden_ref[:, at : at + depth], down_buf[index], preferred_element_type=jnp.float32
             )
             total = term if total is None else total + term
-            at, index = at + depth, index + 1
-    out_ref[...] = total.astype(out_ref.dtype)
-
-
-def result_part(hiddens, downs):
-    rows, columns = hiddens[0].shape[0], downs[0].shape[1]
-    depth = sum(down.shape[0] for down in downs)
+            index += 1
+    length = outs[0].shape[0]
+    for index, out_ref in enumerate(outs):
+        out_ref[...] = total[index * length : (index + 1) * length].astype(out_ref.dtype)
+
+
+def result_part(hiddens, downs, parts):
+    rows, (depth, columns) = hiddens[0].shape[0], downs[0].shape
     return pl.pallas_call(
-        lambda *refs: result_kernel(len(hiddens), *refs),
-        out_shape=jax.ShapeDtypeStruct((rows, columns), jnp.bfloat16),
-        in_specs=[pl.BlockSpec(memory_space=pltpu.VMEM)] * (len(hiddens) + len(downs)),
-        out_specs=pl.BlockSpec(memory_space=pltpu.VMEM),
+        lambda *refs: result_kernel(len(hiddens), len(downs), parts, *refs),
+        out_shape=[jax.ShapeDtypeStruct((rows // parts, columns), jnp.bfloat16)] * parts,
+        in_specs=[pl.BlockSpec(memory_space=pltpu.VMEM)] * len(hiddens)
+        + [pl.BlockSpec(memory_space=pl.ANY)] * len(downs),
+        out_specs=[pl.BlockSpec(memory_space=pltpu.VMEM)] * parts,
+        scratch_shapes=[
+            pltpu.VMEM((len(downs), depth, columns), jnp.bfloat16),
+            pltpu.SemaphoreType.DMA((len(downs),)),
+        ],
         cost_estimate=pl.CostEstimate(
-            flops=2 * rows * depth * columns, bytes_accessed=2 * depth * columns, transcendentals=0
+            flops=2 * rows * depth * len(downs) * columns,
+            bytes_accessed=2 * depth * len(downs) * columns,
+            transcendentals=0,
         ),
     )(*hiddens, *downs)
+
+
+def pooled_rows(mixer_input, mixer_gain, pool_in):
+    normed = norm_rows(mixer_input, mixer_gain)
+    pooled_in = jnp.dot(normed, pool_in, preferred_element_type=jnp.float32).astype(jnp.bfloat16)
+    border = passed_along(pooled_in[pooled_in.shape[0] - RIM :], "ep", 1)
+    return pooled_in, border
 
 
 def on_device(
@@ -210,22 +249,38 @@
         earlier.astype(jnp.bfloat16), either.astype(jnp.bfloat16), preferred_element_type=jnp.float32
     ).astype(jnp.int32)
     place = jnp.where(either, before, -1)
+    ep_place = lax.axis_index("ep")
+    direct = ep_count <= 8 and held == 1 and ep_count & (ep_count - 1) == 0
+    order = expert_ids[0] ^ ep_place if direct else expert_ids[0]
+    block_of = expert_ids ^ ep_place if direct else expert_ids
+    wanted = jnp.sum(
+        jnp.where(order[:, None, None] == expert_ids[:, :, None], place.T[None, :, :], 0), axis=1
+    )
     select = (
-        place.T[:, None, :] == jnp.arange(slots, dtype=jnp.int32)[None, :, None]
+        wanted[:, None, :] == jnp.arange(slots, dtype=jnp.int32)[None, :, None]
     ).astype(jnp.bfloat16)
     sending = jnp.dot(
         select.reshape(experts * slots, block_len), own_rows, preferred_element_type=jnp.float32
     ).astype(jnp.bfloat16)
-    arrived = lax.all_to_all(sending, "ep", split_axis=0, concat_axis=0, tiled=True)
-
-    mixer_partial = mixer_half(mixer_input, mixer_gain, pool_in, pool_map, pool_scale, pool_out)
-    mixer_partial, far_gate, far_up = lax.optimization_barrier((mixer_partial, far_gate, far_up))
+    ranks = sorted(range(1, ep_count), key=lambda k: (-bin(k).count("1"), -k))
+
+    def exchanged(pieces):
+        came = [pieces[0]] + [None] * (ep_count - 1)
+        for k in ranks:
+            came[k] = swapped(pieces[k], "ep", k)
+        return came
+
+    if direct:
+        arrived = exchanged([sending[k * slots : (k + 1) * slots] for k in range(ep_count)])
+        rows = [arrived]
+    else:
+        arrived = lax.all_to_all(sending, "ep", split_axis=0, concat_axis=0, tiled=True)
+        portions = arrived.reshape(ep_count, held, slots, model)
+        rows = [[portions[:, own].reshape(ep_count * slots, model)] for own in range(held)]
+
+    pooled_in, border = pooled_rows(mixer_input, mixer_gain, pool_in)
     far_gates = spread(far_gate, near_masks)
     far_ups = spread(far_up, near_masks)
-    mixer_output = scattered_sum(mixer_partial)
-
-    portions = arrived.reshape(ep_count, held, slots, model)
-    rows = [portions[:, own].reshape(ep_count * slots, model) for own in range(held)]
     near_hidden = [
         hidden_part(rows[own], [w[own] for w in near_gates], [w[own] for w in near_ups])
         for own in range(held)
@@ -237,25 +292,30 @@
     ]
     last, returned = far_hidden, []
     for part in range(parts):
-        last, far_down = lax.optimization_barrier((last, far_downs[part]))
         if part == 0:
-            far_hidden = last
+            far_hidden, far_down = lax.optimization_barrier((last, far_downs[part]))
+        else:
+            far_down, mixer_partial = lax.optimization_barrier((far_downs[part], mixer_partial))
+            mixer_output = scattered_sum(mixer_partial)
         downs = near_downs[part] + spread(far_down, near_masks)
         last = [
-            result_part([near_hidden[own], far_hidden[own]], [w[own] for w in downs])
+            result_part(
+                [near_hidden[own], far_hidden[own]], [w[own] for w in downs], len(rows[own])
+            )
             for own in range(held)
         ]
-        shaped = [value.reshape(ep_count, 1, slots, columns) for value in last]
-        joined = shaped[0] if held == 1 else jnp.concatenate(shaped, axis=1)
-        returned.append(
-            lax.all_to_all(
-                joined.reshape(ep_count * held * slots, columns),
-                "ep",
-                split_axis=0,
-                concat_axis=0,
-                tiled=True,
-            )
-        )
+        if part == 0:
+            last, border = lax.optimization_barrier((last, border))
+            mixer_partial = mixer_half(pooled_in, border, pool_map, pool_scale, pool_out)
+        if part and direct:
+            returned[-1], _ = lax.optimization_barrier((returned[-1], last))
+        if direct:
+            returned.append(exchanged(last[0]))
+        else:
+            shaped = [value[0].reshape(ep_count, 1, slots, columns) for value in last]
+            joined = shaped[0] if held == 1 else jnp.concatenate(shaped, axis=1)
+            joined = joined.reshape(ep_count * held * slots, columns)
+            returned.append([lax.all_to_all(joined, "ep", split_axis=0, concat_axis=0, tiled=True)])
 
     weights = expert_weights(
         own_rows, group_router, expert_router, [hot.astype(jnp.float32) for hot in named]
@@ -263,10 +323,11 @@
     slot_ids = jnp.arange(experts * slots, dtype=jnp.int32)[None, :]
     picks = []
     for hot in named:
-        target = jnp.sum(jnp.where(hot, expert_ids * slots + before, 0), axis=1, keepdims=True)
+        target = jnp.sum(jnp.where(hot, block_of * slots + before, 0), axis=1, keepdims=True)
         picks.append((target == slot_ids).astype(jnp.bfloat16))
     outputs = []
-    for value in returned:
+    for came in returned:
+        value = jnp.concatenate(came, axis=0)
         combined = None
         for pick, weight in zip(picks, weights):
             term = jnp.dot(pick, value, preferred_element_type=jnp.float32) * weight

time: 139 us -> 160 us (1.15)
  the two profiles are of different devices: /device:TPU:0 before, /device:TPU:10 now
where the time goes in v1:
time: 160 us; the launch traced here: 159 us
  waiting for transfers between devices  66.4 us (42%)
  starting transfers between devices  41.3 us (26%)
  Pallas kernels  21.6 us (14%)
  matrix products  13.4 us (8%)
  local copies, waits for them, and re-layouts  9.52 us (6%)
  other arithmetic  5.74 us (4%)
    ppermute x35, waiting for transfers between devices, swapped(): lax.ppermute(value, axis, [(source, source ^ mask) for source in range(co...  66.4 us
    ppermute x35, starting transfers between devices, swapped(): lax.ppermute(value, axis, [(source, source ^ mask) for source in range(co...  37.7 us
    pallas_call x2, Pallas kernels, hidden_part(): pl.pallas_call(lambda *refs: hidden_kernel(parts, count, *refs), out_shap...  13.1 us
    pallas_call x2, Pallas kernels, result_part(): pl.pallas_call(lambda *refs: result_kernel(len(hiddens), len(downs), part...  8.5 us
    dot_general x1, matrix products, mixer_half(): jnp.dot(mixed_rows, pool_out, preferred_element_type=jnp.float32)  7.68 us
    unnamed x64, local copies, waits for them, and re-layouts  3.62 us
    ppermute x1, starting transfers between devices, passed_along(): lax.ppermute(value, axis, [(source, source + steps) for source in range(l...  3.6 us
  transfers between devices with their start and end apart: 36, of which 14 were waited for; matrix products, arithmetic and copies ran while one was open for 17% of the time, Pallas kernels for 14%

profile of v1, /device:TPU:10, one launch (start us, length us, event | category | flops | bytes accessed | tf_op | source)
XLA Modules:
  0.0 159.1 jit_solution(12890434615198719296)
XLA Ops:
  12.1 3.4 %collective-permute-done.1.refs_1_ = bf16[48,2048]{1,0:T(8,128)(2,1)S(1)} collective-permute-done((bf16[48,2048]{1,0:T(8,128)(2,1)S(1)}, bf16[48,2048]{1,0:T(8,128)(2,1)S(1)}, u32[]{:S(2)}, u32[]{:S(2)}) %collective-permute-start.1) | collective-permute-done | bytes 196640 | tf_op jit(solution)/shard_map/ppermute | solution.py:21
  15.5 2.6 %collective-permute-start.4 = (bf16[48,2048]{1,0:T(8,128)(2,1)S(1)}, bf16[48,2048]{1,0:T(8,128)(2,1)S(1)}, u32[]{:S(2)}, u32[]{:S(2)}) collective-permute-start(bf16[48,2048]{1,0:T(8,128)(2,1)S(1)} %get-tuple-element.93), channel_id=1, source_target_pairs={{0,16},{4,20},{8,24},{12,28},{16,0},{20,4},{24,8},{28,12},{1,17},{... | collective-permute-start | bytes 589832 | tf_op jit(solution)/shard_map/ppermute | solution.py:21
  18.1 4.2 %collective-permute-done.3.refs_3_ = bf16[48,2048]{1,0:T(8,128)(2,1)S(1)} collective-permute-done((bf16[48,2048]{1,0:T(8,128)(2,1)S(1)}, bf16[48,2048]{1,0:T(8,128)(2,1)S(1)}, u32[]{:S(2)}, u32[]{:S(2)}) %collective-permute-start.3) | collective-permute-done | bytes 196640 | tf_op jit(solution)/shard_map/ppermute | solution.py:21
  22.3 3.0 %collective-permute-done.4.refs_4_ = bf16[48,2048]{1,0:T(8,128)(2,1)S(1)} collective-permute-done((bf16[48,2048]{1,0:T(8,128)(2,1)S(1)}, bf16[48,2048]{1,0:T(8,128)(2,1)S(1)}, u32[]{:S(2)}, u32[]{:S(2)}) %collective-permute-start.4) | collective-permute-done | bytes 196640 | tf_op jit(solution)/shard_map/ppermute | solution.py:21
  25.3 3.3 %collective-permute-start.5 = (bf16[48,2048]{1,0:T(8,128)(2,1)S(1)}, bf16[48,2048]{1,0:T(8,128)(2,1)S(1)}, u32[]{:S(2)}, u32[]{:S(2)}) collective-permute-start(bf16[48,2048]{1,0:T(8,128)(2,1)S(1)} %get-tuple-element.92), channel_id=1, source_target_pairs={{0,20},{4,16},{8,28},{12,24},{16,4},{20,0},{24,12},{28,8},{1,21},{... | collective-permute-start | bytes 589832 | tf_op jit(solution)/shard_map/ppermute | solution.py:21
  30.2 4.3 %collective-permute-done.5.refs_5_ = bf16[48,2048]{1,0:T(8,128)(2,1)S(1)} collective-permute-done((bf16[48,2048]{1,0:T(8,128)(2,1)S(1)}, bf16[48,2048]{1,0:T(8,128)(2,1)S(1)}, u32[]{:S(2)}, u32[]{:S(2)}) %collective-permute-start.5) | collective-permute-done | bytes 196640 | tf_op jit(solution)/shard_map/ppermute | solution.py:21
  35.0 13.4 %collective-permute-done.12 = bf16[1,2048,256]{2,1,0:T(8,128)(2,1)} collective-permute-done((bf16[1,2048,256]{2,1,0:T(8,128)(2,1)}, bf16[1,2048,256]{2,1,0:T(8,128)(2,1)}, u32[]{:S(2)}, u32[]{:S(2)}) %collective-permute-start.12) | collective-permute-done | bytes 1048608 | tf_op jit(solution)/shard_map/ppermute | solution.py:21
  49.6 2.5 %collective-permute-start.7 = (bf16[48,2048]{1,0:T(8,128)(2,1)S(1)}, bf16[48,2048]{1,0:T(8,128)(2,1)S(1)}, u32[]{:S(2)}, u32[]{:S(2)}) collective-permute-start(bf16[48,2048]{1,0:T(8,128)(2,1)S(1)} %get-tuple-element.90), channel_id=1, source_target_pairs={{0,28},{4,24},{8,20},{12,16},{16,12},{20,8},{24,4},{28,0},{1,29},{... | collective-permute-start | bytes 589832 | tf_op jit(solution)/shard_map/ppermute | solution.py:21
  52.1 9.9 %collective-permute-done.7.refs_7_ = bf16[48,2048]{1,0:T(8,128)(2,1)S(1)} collective-permute-done((bf16[48,2048]{1,0:T(8,128)(2,1)S(1)}, bf16[48,2048]{1,0:T(8,128)(2,1)S(1)}, u32[]{:S(2)}, u32[]{:S(2)}) %collective-permute-start.7) | collective-permute-done | bytes 196640 | tf_op jit(solution)/shard_map/ppermute | solution.py:21
  66.4 6.5 %shard_map.149.refs_0_ = bf16[384,512]{1,0:T(8,128)(2,1)} custom-call(bf16[48,2048]{1,0:T(8,128)(2,1)} %get-tuple-element.97.refs_0_, bf16[48,2048]{1,0:T(8,128)(2,1)} %copy-done.5, bf16[48,2048]{1,0:T(8,128)(2,1)} %copy-done.6, bf16[48,2048]{1,0:T(8,128)(2,1)} %copy-done.7, bf16[48,2048]{1,0:T(8,128)(2,1)} %copy-done.8, bf16[48,2048]{1,0:T(8,128)(2,1)} %copy-done.9, ...), custom_call_target="tpu_custom_call" | custom-call | flops 1610612736 | bytes 4194304 | tf_op jit(solution)/shard_map/pallas_call | solution.py:132
  73.2 3.6 %collective-permute-start.17 = (bf16[15,256]{1,0:T(8,128)(2,1)S(1)}, bf16[15,256]{1,0:T(8,128)(2,1)S(1)}, u32[]{:S(2)}, u32[]{:S(2)}) collective-permute-start(bf16[15,256]{1,0:T(8,128)(2,1)S(1)} %slice.141), channel_id=1, source_target_pairs={{0,4},{4,8},{8,12},{12,16},{16,20},{20,24},{24,28},{1,5},{5,9},{9,... | collective-permute-start | bytes 23048 | tf_op jit(solution)/shard_map/ppermute | solution.py:16
  76.8 6.6 %shard_map.150.refs_1_ = bf16[384,512]{1,0:T(8,128)(2,1)} custom-call(bf16[48,2048]{1,0:T(8,128)(2,1)} %get-tuple-element.97.refs_0_, bf16[48,2048]{1,0:T(8,128)(2,1)} %copy-done.5, bf16[48,2048]{1,0:T(8,128)(2,1)} %copy-done.6, bf16[48,2048]{1,0:T(8,128)(2,1)} %copy-done.7, bf16[48,2048]{1,0:T(8,128)(2,1)} %copy-done.8, bf16[48,2048]{1,0:T(8,128)(2,1)} %copy-done.9, ...), custom_call_target="tpu_custom_call" | custom-call | flops 1610612736 | bytes 4194304 | tf_op jit(solution)/shard_map/pallas_call | solution.py:132
  85.7 4.3 %shard_map.151 = (bf16[48,1024]{1,0:T(8,128)(2,1)}, bf16[48,1024]{1,0:T(8,128)(2,1)}, bf16[48,1024]{1,0:T(8,128)(2,1)}, bf16[48,1024]{1,0:T(8,128)(2,1)}, bf16[4...) custom-call(bf16[384,512]{1,0:T(8,128)(2,1)} %shard_map.149.refs_0_, ...), custom_call_target="tpu_custom_call" | custom-call | flops 805306368 | bytes 2097152 | tf_op jit(solution)/shard_map/pallas_call | solution.py:177
  90.9 7.7 %convolution_convert_fusion = bf16[512,2048]{1,0:T(8,128)(2,1)S(1)} fusion(bf16[256,2048]{1,0:T(8,128)(2,1)S(1)} %copy-done, f32[256]{0:T(256)S(1)} %convert_element_type.186, f32[527,256]{1,0:T(8,128)} %maximum_convert_fusion, f32[512]{0:T(512)S(1)} %minimum_convert_fusion, f32[]{:T(128)S(6)} %convert_element_type.183, f32[]{:T(128)S(6)} %convert_element_type.182, ...), kind=kOutput, calls=%fused_computation.5 | convolution fusion | flops 609746944 | bytes 11668544 | tf_op jit(solution)/shard_map/dot_general | solution.py:77
  104.6 2.2 %collective-permute-start.24 = (bf16[48,1024]{1,0:T(8,128)(2,1)}, bf16[48,1024]{1,0:T(8,128)(2,1)}, u32[]{:S(2)}, u32[]{:S(2)}) collective-permute-start(bf16[48,1024]{1,0:T(8,128)(2,1)} %get-tuple-element.66), channel_id=1, source_target_pairs={{0,20},{4,16},{8,28},{12,24},{16,4},{20,0},{24,12},{28,8},{1,21},{... | collective-permute-start | bytes 294920 | tf_op jit(solution)/shard_map/ppermute | solution.py:21
  109.9 4.2 %shard_map.152 = (bf16[48,1024]{1,0:T(8,128)(2,1)}, bf16[48,1024]{1,0:T(8,128)(2,1)}, bf16[48,1024]{1,0:T(8,128)(2,1)}, bf16[48,1024]{1,0:T(8,128)(2,1)}, bf16[4...) custom-call(bf16[384,512]{1,0:T(8,128)(2,1)} %shard_map.149.refs_0_, ...), custom_call_target="tpu_custom_call" | custom-call | flops 805306368 | bytes 2097152 | tf_op jit(solution)/shard_map/pallas_call | solution.py:177
  117.7 3.4 %collective-permute-start.30 = (bf16[48,1024]{1,0:T(8,128)(2,1)}, bf16[48,1024]{1,0:T(8,128)(2,1)S(1)}, u32[]{:S(2)}, u32[]{:S(2)}) collective-permute-start(bf16[48,1024]{1,0:T(8,128)(2,1)} %get-tuple-element.72), channel_id=1, source_target_pairs={{0,8},{4,12},{8,0},{12,4},{16,24},{20,28},{24,16},{28,20},{1,9},{5... | collective-permute-start | bytes 294920 | tf_op jit(solution)/shard_map/ppermute | solution.py:21
  121.1 2.3 %collective-permute-done.26 = bf16[48,1024]{1,0:T(8,128)(2,1)} collective-permute-done((bf16[48,1024]{1,0:T(8,128)(2,1)}, bf16[48,1024]{1,0:T(8,128)(2,1)}, u32[]{:S(2)}, u32[]{:S(2)}) %collective-permute-start.26) | collective-permute-done | bytes 98336 | tf_op jit(solution)/shard_map/ppermute | solution.py:21
  128.5 2.1 %collective-permute-start.33 = (bf16[48,1024]{1,0:T(8,128)(2,1)S(1)}, bf16[48,1024]{1,0:T(8,128)(2,1)S(1)}, u32[]{:S(2)}, u32[]{:S(2)}) collective-permute-start(bf16[48,1024]{1,0:T(8,128)(2,1)S(1)} %copy-done.21), channel_id=1, source_target_pairs={{0,20},{4,16},{8,28},{12,24},{16,4},{20,0},{24,12},{28,8},{1,21},{... | collective-permute-start | bytes 294920 | tf_op jit(solution)/shard_map/ppermute | solution.py:21
  132.1 1.9 %collective-permute-start.35 = (bf16[48,1024]{1,0:T(8,128)(2,1)S(1)}, bf16[48,1024]{1,0:T(8,128)(2,1)S(1)}, u32[]{:S(2)}, u32[]{:S(2)}) collective-permute-start(bf16[48,1024]{1,0:T(8,128)(2,1)S(1)} %copy-done.19), channel_id=1, source_target_pairs={{0,28},{4,24},{8,20},{12,16},{16,12},{20,8},{24,4},{28,0},{1,29},{... | collective-permute-start | bytes 294920 | tf_op jit(solution)/shard_map/ppermute | solution.py:21
  134.0 4.9 %collective-permute-done.33 = bf16[48,1024]{1,0:T(8,128)(2,1)S(1)} collective-permute-done((bf16[48,1024]{1,0:T(8,128)(2,1)S(1)}, bf16[48,1024]{1,0:T(8,128)(2,1)S(1)}, u32[]{:S(2)}, u32[]{:S(2)}) %collective-permute-start.33) | collective-permute-done | bytes 98336 | tf_op jit(solution)/shard_map/ppermute | solution.py:21
  138.9 3.2 %collective-permute-done.34 = bf16[48,1024]{1,0:T(8,128)(2,1)S(1)} collective-permute-done((bf16[48,1024]{1,0:T(8,128)(2,1)S(1)}, bf16[48,1024]{1,0:T(8,128)(2,1)S(1)}, u32[]{:S(2)}, u32[]{:S(2)}) %collective-permute-start.34) | collective-permute-done | bytes 98336 | tf_op jit(solution)/shard_map/ppermute | solution.py:21
  142.1 2.3 %collective-permute-done.35 = bf16[48,1024]{1,0:T(8,128)(2,1)S(1)} collective-permute-done((bf16[48,1024]{1,0:T(8,128)(2,1)S(1)}, bf16[48,1024]{1,0:T(8,128)(2,1)S(1)}, u32[]{:S(2)}, u32[]{:S(2)}) %collective-permute-start.35) | collective-permute-done | bytes 98336 | tf_op jit(solution)/shard_map/ppermute | solution.py:21
  146.9 11.3 %collective-permute-done.19 = bf16[1,128,2048]{2,1,0:T(8,128)(2,1)S(1)} collective-permute-done((bf16[1,128,2048]{2,1,0:T(8,128)(2,1)S(1)}, bf16[1,128,2048]{2,1,0:T(8,128)(2,1)S(1)}, u32[]{:S(2)}, u32[]{:S(2)}) %collective-permute-start.19) | collective-permute-done | bytes 524320 | tf_op jit(solution)/shard_map/ppermute | solution.py:21
  (158 shorter events, 44.8 us)
Async XLA Ops:
  0.6 34.3 %collective-permute-start.10 = (bf16[1,2048,256]{2,1,0:T(8,128)(2,1)}, bf16[1,2048,256]{2,1,0:T(8,128)(2,1)}, u32[]{:S(2)}, u32[]{:S(2)}) collective-permute-start(bf16[1,2048,256]{2,1,0:T(8,128)(2,1)} %param.25), channel_id=1, source_target_pairs={{0,2},{1,3},{2,0},{3,1},{4,6},{5,7},{6,4},{7,5},{8,10},{9,11},{10,... | collective-permute-start | bytes 3145736 | tf_op jit(solution)/shard_map/ppermute | solution.py:21
  1.2 47.1 %collective-permute-start.12 = (bf16[1,2048,256]{2,1,0:T(8,128)(2,1)}, bf16[1,2048,256]{2,1,0:T(8,128)(2,1)}, u32[]{:S(2)}, u32[]{:S(2)}) collective-permute-start(bf16[1,2048,256]{2,1,0:T(8,128)(2,1)} %param.26), channel_id=1, source_target_pairs={{0,2},{1,3},{2,0},{3,1},{4,6},{5,7},{6,4},{7,5},{8,10},{9,11},{10,... | collective-permute-start | bytes 3145736 | tf_op jit(solution)/shard_map/ppermute | solution.py:21
  10.6 11.8 %collective-permute-start.3 = (bf16[48,2048]{1,0:T(8,128)(2,1)S(1)}, bf16[48,2048]{1,0:T(8,128)(2,1)S(1)}, u32[]{:S(2)}, u32[]{:S(2)}) collective-permute-start(bf16[48,2048]{1,0:T(8,128)(2,1)S(1)} %get-tuple-element.94), channel_id=1, source_target_pairs={{0,12},{4,8},{8,4},{12,0},{16,28},{20,24},{24,20},{28,16},{1,13},{... | collective-permute-start | bytes 589832 | tf_op jit(solution)/shard_map/ppermute | solution.py:21
  18.1 46.7 %collective-permute-start.8 = (bf16[1,2048,256]{2,1,0:T(8,128)(2,1)S(1)}, bf16[1,2048,256]{2,1,0:T(8,128)(2,1)}, u32[]{:S(2)}, u32[]{:S(2)}) collective-permute-start(bf16[1,2048,256]{2,1,0:T(8,128)(2,1)S(1)} %copy-done.3), channel_id=1, source_target_pairs={{0,1},{1,0},{2,3},{3,2},{4,5},{5,4},{6,7},{7,6},{8,9},{9,8},{10,11... | collective-permute-start | bytes 3145736 | tf_op jit(solution)/shard_map/ppermute | solution.py:21
  22.3 42.5 %collective-permute-start.9 = (bf16[1,2048,256]{2,1,0:T(8,128)(2,1)S(1)}, bf16[1,2048,256]{2,1,0:T(8,128)(2,1)}, u32[]{:S(2)}, u32[]{:S(2)}) collective-permute-start(bf16[1,2048,256]{2,1,0:T(8,128)(2,1)S(1)} %copy-done.4), channel_id=1, source_target_pairs={{0,1},{1,0},{2,3},{3,2},{4,5},{5,4},{6,7},{7,6},{8,9},{9,8},{10,11... | collective-permute-start | bytes 3145736 | tf_op jit(solution)/shard_map/ppermute | solution.py:21
  34.5 14.4 %collective-permute-start.6 = (bf16[48,2048]{1,0:T(8,128)(2,1)S(1)}, bf16[48,2048]{1,0:T(8,128)(2,1)S(1)}, u32[]{:S(2)}, u32[]{:S(2)}) collective-permute-start(bf16[48,2048]{1,0:T(8,128)(2,1)S(1)} %get-tuple-element.91), channel_id=1, source_target_pairs={{0,24},{4,28},{8,16},{12,20},{16,8},{20,12},{24,0},{28,4},{1,25},{... | collective-permute-start | bytes 589832 | tf_op jit(solution)/shard_map/ppermute | solution.py:21
  35.0 38.0 %collective-permute-start.11 = (bf16[1,2048,256]{2,1,0:T(8,128)(2,1)}, bf16[1,2048,256]{2,1,0:T(8,128)(2,1)}, u32[]{:S(2)}, u32[]{:S(2)}) collective-permute-start(bf16[1,2048,256]{2,1,0:T(8,128)(2,1)} %collective-permute-done.10), channel_id=1, source_target_pairs={{0,1},{1,0},{2,3},{3,2},{4,5},{5,4},{6,7},{7,6},{8,9},{9,8},{10,11... | collective-permute-start | bytes 3145736 | tf_op jit(solution)/shard_map/ppermute | solution.py:21
  48.4 24.8 %collective-permute-start.13 = (bf16[1,2048,256]{2,1,0:T(8,128)(2,1)}, bf16[1,2048,256]{2,1,0:T(8,128)(2,1)}, u32[]{:S(2)}, u32[]{:S(2)}) collective-permute-start(bf16[1,2048,256]{2,1,0:T(8,128)(2,1)} %collective-permute-done.12), channel_id=1, source_target_pairs={{0,1},{1,0},{2,3},{3,2},{4,5},{5,4},{6,7},{7,6},{8,9},{9,8},{10,11... | collective-permute-start | bytes 3145736 | tf_op jit(solution)/shard_map/ppermute | solution.py:21
  49.6 12.4 %collective-permute-start.7 = (bf16[48,2048]{1,0:T(8,128)(2,1)S(1)}, bf16[48,2048]{1,0:T(8,128)(2,1)S(1)}, u32[]{:S(2)}, u32[]{:S(2)}) collective-permute-start(bf16[48,2048]{1,0:T(8,128)(2,1)S(1)} %get-tuple-element.90), channel_id=1, source_target_pairs={{0,28},{4,24},{8,20},{12,16},{16,12},{20,8},{24,4},{28,0},{1,29},{... | collective-permute-start | bytes 589832 | tf_op jit(solution)/shard_map/ppermute | solution.py:21
  62.0 21.4 %collective-permute-start.14 = (bf16[1,256,1024]{2,1,0:T(8,128)(2,1)}, bf16[1,256,1024]{2,1,0:T(8,128)(2,1)}, u32[]{:S(2)}, u32[]{:S(2)}) collective-permute-start(bf16[1,256,1024]{2,1,0:T(8,128)(2,1)} %get-tuple-element.100), channel_id=1, source_target_pairs={{0,2},{1,3},{2,0},{3,1},{4,6},{5,7},{6,4},{7,5},{8,10},{9,11},{10,... | collective-permute-start | bytes 1572872 | tf_op jit(solution)/shard_map/ppermute | solution.py:21
  64.8 19.4 %collective-permute-start.15 = (bf16[1,256,1024]{2,1,0:T(8,128)(2,1)}, bf16[1,256,1024]{2,1,0:T(8,128)(2,1)}, u32[]{:S(2)}, u32[]{:S(2)}) collective-permute-start(bf16[1,256,1024]{2,1,0:T(8,128)(2,1)} %get-tuple-element.100), channel_id=1, source_target_pairs={{0,1},{1,0},{2,3},{3,2},{4,5},{5,4},{6,7},{7,6},{8,9},{9,8},{10,11... | collective-permute-start | bytes 1572872 | tf_op jit(solution)/shard_map/ppermute | solution.py:21
  64.9 33.7 %collective-permute-start = (bf16[1,256,1024]{2,1,0:T(8,128)(2,1)}, bf16[1,256,1024]{2,1,0:T(8,128)(2,1)}, u32[]{:S(2)}, u32[]{:S(2)}) collective-permute-start(bf16[1,256,1024]{2,1,0:T(8,128)(2,1)} %get-tuple-element.101), channel_id=1, source_target_pairs={{0,2},{1,3},{2,0},{3,1},{4,6},{5,7},{6,4},{7,5},{8,10},{9,11},{10,... | collective-permute-start | bytes 1572872 | tf_op jit(solution)/shard_map/ppermute | solution.py:21
  72.9 30.0 %collective-permute-start.27 = (bf16[1,256,1024]{2,1,0:T(8,128)(2,1)}, bf16[1,256,1024]{2,1,0:T(8,128)(2,1)}, u32[]{:S(2)}, u32[]{:S(2)}) collective-permute-start(bf16[1,256,1024]{2,1,0:T(8,128)(2,1)} %get-tuple-element.101), channel_id=1, source_target_pairs={{0,1},{1,0},{2,3},{3,2},{4,5},{5,4},{6,7},{7,6},{8,9},{9,8},{10,11... | collective-permute-start | bytes 1572872 | tf_op jit(solution)/shard_map/ppermute | solution.py:21
  73.2 16.9 %collective-permute-start.17 = (bf16[15,256]{1,0:T(8,128)(2,1)S(1)}, bf16[15,256]{1,0:T(8,128)(2,1)S(1)}, u32[]{:S(2)}, u32[]{:S(2)}) collective-permute-start(bf16[15,256]{1,0:T(8,128)(2,1)S(1)} %slice.141), channel_id=1, source_target_pairs={{0,4},{4,8},{8,12},{12,16},{16,20},{20,24},{24,28},{1,5},{5,9},{9,... | collective-permute-start | bytes 23048 | tf_op jit(solution)/shard_map/ppermute | solution.py:16
  101.4 12.7 %collective-permute-start.22 = (bf16[48,1024]{1,0:T(8,128)(2,1)}, bf16[48,1024]{1,0:T(8,128)(2,1)S(1)}, u32[]{:S(2)}, u32[]{:S(2)}) collective-permute-start(bf16[48,1024]{1,0:T(8,128)(2,1)} %get-tuple-element.64), channel_id=1, source_target_pairs={{0,12},{4,8},{8,4},{12,0},{16,28},{20,24},{24,20},{28,16},{1,13},{... | collective-permute-start | bytes 294920 | tf_op jit(solution)/shard_map/ppermute | solution.py:21
  104.6 13.1 %collective-permute-start.24 = (bf16[48,1024]{1,0:T(8,128)(2,1)}, bf16[48,1024]{1,0:T(8,128)(2,1)}, u32[]{:S(2)}, u32[]{:S(2)}) collective-permute-start(bf16[48,1024]{1,0:T(8,128)(2,1)} %get-tuple-element.66), channel_id=1, source_target_pairs={{0,20},{4,16},{8,28},{12,24},{16,4},{20,0},{24,12},{28,8},{1,21},{... | collective-permute-start | bytes 294920 | tf_op jit(solution)/shard_map/ppermute | solution.py:21
  106.8 14.3 %collective-permute-start.25 = (bf16[48,1024]{1,0:T(8,128)(2,1)}, bf16[48,1024]{1,0:T(8,128)(2,1)}, u32[]{:S(2)}, u32[]{:S(2)}) collective-permute-start(bf16[48,1024]{1,0:T(8,128)(2,1)} %get-tuple-element.67), channel_id=1, source_target_pairs={{0,24},{4,28},{8,16},{12,20},{16,8},{20,12},{24,0},{28,4},{1,25},{... | collective-permute-start | bytes 294920 | tf_op jit(solution)/shard_map/ppermute | solution.py:21
  107.5 15.9 %collective-permute-start.26 = (bf16[48,1024]{1,0:T(8,128)(2,1)}, bf16[48,1024]{1,0:T(8,128)(2,1)}, u32[]{:S(2)}, u32[]{:S(2)}) collective-permute-start(bf16[48,1024]{1,0:T(8,128)(2,1)} %get-tuple-element.68), channel_id=1, source_target_pairs={{0,28},{4,24},{8,20},{12,16},{16,12},{20,8},{24,4},{28,0},{1,29},{... | collective-permute-start | bytes 294920 | tf_op jit(solution)/shard_map/ppermute | solution.py:21
  114.1 30.3 %collective-permute-start.18 = (bf16[2,128,2048]{2,1,0:T(8,128)(2,1)}, bf16[2,128,2048]{2,1,0:T(8,128)(2,1)S(1)}, u32[]{:S(2)}, u32[]{:S(2)}) collective-permute-start(bf16[2,128,2048]{2,1,0:T(8,128)(2,1)} %dynamic-slice_bitcast_fusion), channel_id=1, source_target_pairs={{0,1},{1,0},{2,3},{3,2},{4,5},{5,4},{6,7},{7,6},{8,9},{9,8},{10,11... | collective-permute-start | bytes 3145736 | tf_op jit(solution)/shard_map/ppermute | solution.py:21
  114.2 14.3 %collective-permute-start.29 = (bf16[48,1024]{1,0:T(8,128)(2,1)}, bf16[48,1024]{1,0:T(8,128)(2,1)S(1)}, u32[]{:S(2)}, u32[]{:S(2)}) collective-permute-start(bf16[48,1024]{1,0:T(8,128)(2,1)} %get-tuple-element.71), channel_id=1, source_target_pairs={{0,4},{4,0},{8,12},{12,8},{16,20},{20,16},{24,28},{28,24},{1,5},{5... | collective-permute-start | bytes 294920 | tf_op jit(solution)/shard_map/ppermute | solution.py:21
  117.7 12.9 %collective-permute-start.30 = (bf16[48,1024]{1,0:T(8,128)(2,1)}, bf16[48,1024]{1,0:T(8,128)(2,1)S(1)}, u32[]{:S(2)}, u32[]{:S(2)}) collective-permute-start(bf16[48,1024]{1,0:T(8,128)(2,1)} %get-tuple-element.72), channel_id=1, source_target_pairs={{0,8},{4,12},{8,0},{12,4},{16,24},{20,28},{24,16},{28,20},{1,9},{5... | collective-permute-start | bytes 294920 | tf_op jit(solution)/shard_map/ppermute | solution.py:21
  130.7 11.5 %collective-permute-start.34 = (bf16[48,1024]{1,0:T(8,128)(2,1)S(1)}, bf16[48,1024]{1,0:T(8,128)(2,1)S(1)}, u32[]{:S(2)}, u32[]{:S(2)}) collective-permute-start(bf16[48,1024]{1,0:T(8,128)(2,1)S(1)} %copy-done.20), channel_id=1, source_target_pairs={{0,24},{4,28},{8,16},{12,20},{16,8},{20,12},{24,0},{28,4},{1,25},{... | collective-permute-start | bytes 294920 | tf_op jit(solution)/shard_map/ppermute | solution.py:21
  132.1 12.4 %collective-permute-start.35 = (bf16[48,1024]{1,0:T(8,128)(2,1)S(1)}, bf16[48,1024]{1,0:T(8,128)(2,1)S(1)}, u32[]{:S(2)}, u32[]{:S(2)}) collective-permute-start(bf16[48,1024]{1,0:T(8,128)(2,1)S(1)} %copy-done.19), channel_id=1, source_target_pairs={{0,28},{4,24},{8,20},{12,16},{16,12},{20,8},{24,4},{28,0},{1,29},{... | collective-permute-start | bytes 294920 | tf_op jit(solution)/shard_map/ppermute | solution.py:21
  144.9 13.3 %collective-permute-start.19 = (bf16[1,128,2048]{2,1,0:T(8,128)(2,1)S(1)}, bf16[1,128,2048]{2,1,0:T(8,128)(2,1)S(1)}, u32[]{:S(2)}, u32[]{:S(2)}) collective-permute-start(bf16[1,128,2048]{2,1,0:T(8,128)(2,1)S(1)} %constant_dynamic-slice_fusion), channel_id=1, source_target_pairs={{0,2},{1,3},{2,0},{3,1},{4,6},{5,7},{6,4},{7,5},{8,10},{9,11},{10,... | collective-permute-start | bytes 1572872 | tf_op jit(solution)/shard_map/ppermute | solution.py:21
  (37 other events, 519.2 us)
